TPU v7x, 32 devices: a whole 2x2x4 slice. The times are simulated.
32 devices in a mesh: grp: 2 (over y), sp: 4 (over z), tp: 4 (over x, core).
Axes of the slice: x: 2, y: 2, z: 4, core: 2. Of those that a mesh axis runs over, the one named last changes fastest.
Arguments:
- query_latent: bfloat16 [1024, 768], P(('grp', 'sp')), parts along dimension 0, may hold values from -6 to 6
- key_latent: bfloat16 [1024, 256], P(('grp', 'sp', 'tp')), parts along dimension 0, may hold values from -20 to 20
- rotary_key: bfloat16 [1024, 64], P(('grp', 'sp', 'tp')), parts along dimension 0, may hold values from -1000 to 1000
- query_gain: float32 [768], replicated, may hold values from 0.1 to 1.9
- latent_gain: float32 [256], replicated, may hold values from 0.1 to 1.9
- query_up: bfloat16 [768, 3072], P(None, 'tp'), may hold values from -0.21875 to 0.21875
- key_up: bfloat16 [256, 2048], P(None, 'tp'), may hold values from -0.375 to 0.375
- value_up: bfloat16 [256, 2048], P(None, 'tp'), may hold values from -0.375 to 0.375
- out_gain: float32 [2048], P('tp'), may hold values from 0.1 to 1.9
- out_weight: bfloat16 [2048, 4096], P('sp', 'tp'), may hold values from -0.125 to 0.125
Outputs:
- mixed: bfloat16 [1024, 4096], P(('grp', 'sp'), 'tp'), parts along dimension 0
There are 2 independent parts, one for each index of `grp`. A program takes and returns all parts, laid end to end along the dimension named above; an argument that names none is the same for every part. Nothing has to cross between parts.
All inputs are finite; a program needn't handle non-finite values.
Results may differ from a plain program's by a relative error of at most 0.02.
The roundings to bfloat16 on the way count: a program that leaves them out, or rounds other values in their place, can miss the bound.
Values may be sent and summed in bfloat16 or wider, within the bound.
A program may use at most 128 MiB of HBM per device.

v0:
```python
import jax
import jax.numpy as jnp
from jax import lax
from jax.sharding import PartitionSpec as P

HEADS = 16
NOPE_DIM = 128
ROPE_DIM = 64
VALUE_DIM = 128
KVRANK = 256
norm_eps = 1e-06
rope_theta = 10000.0


def rms_scaled(inputs, gain_vec):
    widened = inputs.astype(jnp.float32)
    return (
        widened
        * lax.rsqrt(jnp.mean(widened * widened, axis=-1, keepdims=True) + norm_eps)
        * gain_vec
    )


def rotate_half(inputs, positions):
    half_width = inputs.shape[-1] // 2
    inverse = rope_theta ** (-jnp.arange(half_width, dtype=jnp.float32) / half_width)
    angles = positions[:, None] * inverse[None, :]
    if inputs.ndim == 3:
        angles = angles[:, None, :]
    cosine = jnp.cos(angles)
    sine = jnp.sin(angles)
    widened = inputs.astype(jnp.float32)
    first = widened[..., :half_width]
    second = widened[..., half_width:]
    return jnp.concatenate(
        [first * cosine - second * sine, second * cosine + first * sine], axis=-1
    )


def on_device(
    query_latent,
    key_latent,
    rotary_key,
    query_gain,
    latent_gain,
    query_up,
    key_up,
    value_up,
    out_gain,
    out_weight,
):
    block_rows = query_latent.shape[0]
    row_count = key_latent.shape[0]
    head_local = key_up.shape[1] // NOPE_DIM
    block_start = lax.axis_index("sp") * block_rows
    own_start = block_start + lax.axis_index("tp") * row_count
    score_scale = (NOPE_DIM + ROPE_DIM) ** (-0.5)
    normed = rms_scaled(query_latent, query_gain).astype(jnp.bfloat16)
    query_full = jnp.dot(normed, query_up, preferred_element_type=jnp.float32).astype(jnp.bfloat16)
    query_full = query_full.reshape(block_rows, head_local, NOPE_DIM + ROPE_DIM)
    query_positions = (block_start + jnp.arange(block_rows, dtype=jnp.int32)).astype(jnp.float32)
    query_plain = query_full[..., :NOPE_DIM]
    query_turned = rotate_half(query_full[..., NOPE_DIM:], query_positions).astype(jnp.bfloat16)
    latent_normed = rms_scaled(key_latent, latent_gain).astype(jnp.bfloat16)
    own_positions = (own_start + jnp.arange(row_count, dtype=jnp.int32)).astype(jnp.float32)
    key_turned = rotate_half(rotary_key, own_positions).astype(jnp.bfloat16)
    running_max = jnp.full((block_rows, head_local), -1e30, jnp.float32)
    running_sum = jnp.zeros((block_rows, head_local), jnp.float32)
    weighted = jnp.zeros((block_rows, head_local, KVRANK), jnp.float32)
    latents = lax.all_gather(latent_normed, ("sp", "tp"), axis=0, tiled=True)
    turned_keys = lax.all_gather(key_turned, ("sp", "tp"), axis=0, tiled=True)
    portion_rows = latents.shape[0]
    step_rows = min(portion_rows, 2048)
    for begin in range(0, portion_rows, step_rows):
        latent_part = latents[begin : begin + step_rows]
        turned_part = turned_keys[begin : begin + step_rows]
        key_plain = jnp.dot(latent_part, key_up, preferred_element_type=jnp.float32).astype(
            jnp.bfloat16
        )
        key_plain = key_plain.reshape(latent_part.shape[0], head_local, NOPE_DIM)
        scores = jnp.einsum(
            "qhd,khd->qhk", query_plain, key_plain, preferred_element_type=jnp.float32
        )
        scores = scores + jnp.einsum(
            "qhd,kd->qhk", query_turned, turned_part, preferred_element_type=jnp.float32
        )
        scores = scores * score_scale
        new_max = jnp.maximum(running_max, jnp.max(scores, axis=-1))
        rescale = jnp.exp(running_max - new_max)
        expo = jnp.exp(scores - new_max[..., None])
        running_sum = running_sum * rescale + jnp.sum(expo, axis=-1)
        weighted = weighted * rescale[..., None] + jnp.einsum(
            "qhk,kc->qhc",
            expo.astype(jnp.bfloat16),
            latent_part,
            preferred_element_type=jnp.float32,
        )
        running_max = new_max
    final_state = (running_max, running_sum, weighted)
    running_max, running_sum, weighted = final_state
    latent_mix = (weighted / running_sum[..., None]).astype(jnp.bfloat16)
    value_heads = value_up.reshape(KVRANK, head_local, VALUE_DIM)
    head_out = jnp.einsum(
        "qhc,chd->qhd", latent_mix, value_heads, preferred_element_type=jnp.float32
    ).astype(jnp.bfloat16)
    head_out = head_out.reshape(block_rows, head_local * VALUE_DIM)
    widened = head_out.astype(jnp.float32)
    square_part = jnp.sum(widened * widened, axis=1)
    gained = (widened * out_gain).astype(jnp.bfloat16)
    all_gained, square_parts = (
        lax.all_gather(gained, "tp", axis=1, tiled=True),
        lax.all_gather(square_part[:, None].astype(jnp.bfloat16), "tp", axis=1, tiled=True).astype(
            jnp.float32
        ),
    )
    all_squares = jnp.sum(square_parts, axis=1)
    own_sums = jnp.dot(
        all_gained,
        lax.all_gather(out_weight, "sp", axis=0, tiled=True),
        preferred_element_type=jnp.float32,
    )
    mean_square = all_squares / (HEADS * VALUE_DIM)
    return (own_sums * lax.rsqrt(mean_square + norm_eps)[:, None]).astype(jnp.bfloat16)


def solution(mesh):
    in_specs = (
        P(("grp", "sp"), None),
        P(("grp", "sp", "tp"), None),
        P(("grp", "sp", "tp"), None),
        P(),
        P(),
        P(None, "tp"),
        P(None, "tp"),
        P(None, "tp"),
        P("tp"),
        P("sp", "tp"),
    )
    out_specs = P(("grp", "sp"), "tp")
    return jax.shard_map(
        on_device, mesh=mesh, in_specs=in_specs, out_specs=out_specs, check_vma=False
    )
```

profile of v0, /device:TPU:0, one launch (start us, length us, event | category | flops | bytes accessed | tf_op | source)
XLA Modules:
  0.0 103.9 jit_solution(13197024730950181628)
XLA Ops:
  6.5 0.0 copy-start
  6.5 0.0 copy-start.1
  6.5 0.0 all-gather.3.cloned.1.call-start
  6.5 0.7 all-gather.3.cloned.1.call-update
  7.3 1.0 %fusion.13 = f32[128]{0:T(128)S(1)} fusion(bf16[128,768]{1,0:T(8,128)(2,1)} %param.10), kind=kLoop, calls=%fused_computation.19 | loop fusion | flops 294784 | bytes 197120 | tf_op jit(solution)/shard_map/reduce_sum | solution.py:19
  8.3 0.0 copy-done
  8.3 1.3 %convolution_convert_fusion.1 = bf16[128,768]{1,0:T(8,128)(2,1)S(1)} fusion(bf16[768,768]{1,0:T(8,128)(2,1)S(1)} %copy-done, bf16[128,768]{1,0:T(8,128)(2,1)} %param.10, f32[768]{0:T(1024)} %param.13, f32[128]{0:T(128)S(1)} %add_rsqrt_fusion.1), kind=kOutput, calls=%fused_computation.9 | convolution fusion | flops 151486464 | bytes 1576448 | tf_op jit(solution)/shard_map/dot_general | solution.py:59
  9.6 0.2 copy.21
  9.8 0.7 convert_element_type.94
  10.5 1.1 %copy.30 = bf16[256,512]{0,1:T(8,128)(2,1)S(1)} copy(bf16[256,512]{1,0:T(8,128)(2,1)} %param.17) | data formatting | bytes 524288 | tf_op jit(solution)/shard_map/reshape | solution.py:102
  11.6 0.1 fusion.37
  11.8 0.1 pad_maximum_fusion
  11.8 24.3 %all_gather.16 = bf16[512,64]{1,0:T(8,128)(2,1)S(1)} all-gather(bf16[32,64]{1,0:T(8,128)(2,1)S(1)} %pad_maximum_fusion), channel_id=1, replica_groups=mesh['grp'=2,'sp'=4,'tp'=4] {'sp','tp'}, dimensions={0}, use_global_device_ids=true | all-gather | bytes 69632 | tf_op jit(solution)/shard_map/all_gather | solution.py:71
  36.2 0.8 fusion.29
  37.0 0.8 fusion.31
  37.8 20.0 %all_gather.15 = bf16[512,256]{1,0:T(8,128)(2,1)S(1)} all-gather(bf16[32,256]{1,0:T(8,128)(2,1)S(1)} %fusion.31), channel_id=1, replica_groups=mesh['grp'=2,'sp'=4,'tp'=4] {'sp','tp'}, dimensions={0}, use_global_device_ids=true | all-gather | bytes 278528 | tf_op jit(solution)/shard_map/all_gather | solution.py:70
  57.9 0.1 multiply_cosine_fusion.1
  58.0 0.0 copy-done.1
  58.1 0.3 convolution_convert_fusion
  58.4 0.0 copy-start.2
  58.4 0.3 convolution_bitcast_fusion
  58.8 0.3 fusion.42
  59.1 0.2 fusion.7
  59.2 0.6 multiply_reduce_fusion
  59.8 5.1 %all-gather = bf16[4,1,128]{2,1,0:T(2,128)(2,1)S(1)} all-gather(bf16[1,1,128]{2,1,0:T(2,128)(2,1)S(1)} %bitcast.36), channel_id=1, replica_groups=mesh['grp'=2,'sp'=4,'tp'=4] {'tp'}, dimensions={0}, use_global_device_ids=true | all-gather | bytes 1280 | tf_op jit(solution)/shard_map/all_gather | solution.py:112
  64.9 0.0 copy-done.2
  64.9 0.1 fusion.16
  65.0 7.3 %all_gather.17 = bf16[128,2048]{0,1:T(8,128)(2,1)S(1)} all-gather(bf16[128,512]{0,1:T(8,128)(2,1)S(1)} %fusion.16), channel_id=1, replica_groups=mesh['grp'=2,'sp'=4,'tp'=4] {'tp'}, dimensions={1}, use_global_device_ids=true | all-gather | bytes 655360 | tf_op jit(solution)/shard_map/all_gather | solution.py:111
  72.3 21.2 %all-gather.3.cloned.1.call-done = bf16[2048,1024]{1,0:T(8,128)(2,1)} async-done(((bf16[512,1024]{1,0:T(8,128)(2,1)}), bf16[2048,1024]{1,0:T(8,128)(2,1)}) %all-gather.3.cloned.1.call-update) | async-done | bytes 4194320 | tf_op jit(solution)/shard_map/all_gather | solution.py:119
  93.5 3.6 %fusion.3 = bf16[128,1024]{1,0:T(8,128)(2,1)} fusion(bf16[128,2048]{0,1:T(8,128)(2,1)S(1)} %all_gather.17, bf16[2048,1024]{1,0:T(8,128)(2,1)} %all-gather.3.cloned.1.call-done, f32[128]{0:T(128)S(1)} %add_rsqrt_fusion), kind=kOutput, calls=%fused_computation.8 | convolution fusion | flops 537133056 | bytes 4981248 | tf_op jit(solution)/shard_map/dot_general | solution.py:117
  (11 shorter events, 0.1 us)
Async XLA Ops:
  6.5 1.8 %copy-start = (bf16[768,768]{1,0:T(8,128)(2,1)S(1)}, bf16[768,768]{1,0:T(8,128)(2,1)}, u32[]{:S(2)}) copy-start(bf16[768,768]{1,0:T(8,128)(2,1)} %param.15) | copy-start | bytes 3538948
  6.5 51.5 %copy-start.1 = (bf16[256,512]{1,0:T(8,128)(2,1)S(1)}, bf16[256,512]{1,0:T(8,128)(2,1)}, u32[]{:S(2)}) copy-start(bf16[256,512]{1,0:T(8,128)(2,1)} %param.16) | copy-start | bytes 786436
  6.5 86.9 %all-gather.3.cloned.1.call-start = ((), (), s32[]{:S(2)}) async-start(), calls=%async_computation | async-start | bytes 5242880 | tf_op jit(solution)/shard_map/all_gather | solution.py:119
  58.4 6.5 %copy-start.2 = (f32[512]{0:T(512)S(1)}, f32[512]{0:T(512)}, u32[]{:S(2)}) copy-start(f32[512]{0:T(512)} %param.18) | copy-start | bytes 6148
Sparse Core Ops, SparseCore 0:
  8.9 84.5 all-gather.2
where the time goes:
time: 104 us
  blocking collectives  56.7 us (55%)
  waiting for transfers between devices  21.9 us (21%)
  between operations  13.5 us (13%)
  matrix products  6.45 us (6%)
  other arithmetic  4.14 us (4%)
  local copies, waits for them, and re-layouts  1.25 us (1%)
    all_gather x1, blocking collectives, on_device(): turned_keys = lax.all_gather(key_turned, ('sp', 'tp'), axis=0, tiled=True)  24.3 us
    all_gather x1, waiting for transfers between devices, on_device(): lax.all_gather(out_weight, 'sp', axis=0, tiled=True)  21.2 us
    all_gather x1, blocking collectives, on_device(): latents = lax.all_gather(latent_normed, ('sp', 'tp'), axis=0, tiled=True)  20 us
    all_gather x1, blocking collectives, on_device(): lax.all_gather(gained, 'tp', axis=1, tiled=True)  7.27 us
    all_gather x1, blocking collectives, on_device(): lax.all_gather(square_part[:, None].astype(jnp.bfloat16), 'tp', axis=1, t...  5.06 us
    dot_general x1, matrix products, on_device(): jnp.dot(all_gained, lax.all_gather(out_weight, 'sp', axis=0, tiled=True),...  3.64 us
  transfers between devices with their start and end apart: 1, of which 1 were waited for; matrix products, arithmetic and copies ran while one was open for 8% of the time, Pallas kernels for 0%

commit v1 on v0

--- a/solution.py
+++ b/solution.py
@@ -10,6 +10,10 @@
 KVRANK = 256
 norm_eps = 1e-06
 rope_theta = 10000.0
+
+
+def resolve_the_plane(frame, link_axis):
+    return jnp.concatenate(jax.lax.all_gather(frame, axis_name=link_axis), 1)
 
 
 def rms_scaled(inputs, gain_vec):
@@ -108,7 +112,7 @@
     square_part = jnp.sum(widened * widened, axis=1)
     gained = (widened * out_gain).astype(jnp.bfloat16)
     all_gained, square_parts = (
-        lax.all_gather(gained, "tp", axis=1, tiled=True),
+        resolve_the_plane(gained, "tp"),
         lax.all_gather(square_part[:, None].astype(jnp.bfloat16), "tp", axis=1, tiled=True).astype(
             jnp.float32
         ),

time: 104 us -> 104 us (level)
  no operation moved by 1% of the time
where the time goes in v1:
time: 104 us
  blocking collectives  56.7 us (55%)
  waiting for transfers between devices  21.5 us (21%)
  between operations  13.5 us (13%)
  matrix products  6.45 us (6%)
  other arithmetic  4.04 us (4%)
  local copies, waits for them, and re-layouts  1.66 us (2%)
    all_gather x1, blocking collectives, on_device(): turned_keys = lax.all_gather(key_turned, ('sp', 'tp'), axis=0, tiled=True)  24.3 us
    all_gather x1, waiting for transfers between devices, on_device(): lax.all_gather(out_weight, 'sp', axis=0, tiled=True)  20.8 us
    all_gather x1, blocking collectives, on_device(): latents = lax.all_gather(latent_normed, ('sp', 'tp'), axis=0, tiled=True)  20 us
    all_gather x1, blocking collectives, resolve_the_plane(): return jnp.concatenate(jax.lax.all_gather(frame, axis_name=link_axis), 1)  7.27 us
    all_gather x1, blocking collectives, on_device(): lax.all_gather(square_part[:, None].astype(jnp.bfloat16), 'tp', axis=1, t...  5.06 us
    dot_general x1, matrix products, on_device(): jnp.dot(all_gained, lax.all_gather(out_weight, 'sp', axis=0, tiled=True),...  3.64 us
  transfers between devices with their start and end apart: 1, of which 1 were waited for; matrix products, arithmetic and copies ran while one was open for 8% of the time, Pallas kernels for 0%

profile of v1, /device:TPU:0, one launch (start us, length us, event | category | flops | bytes accessed | tf_op | source)
XLA Modules:
  0.0 103.9 jit_solution(3047194498151082465)
XLA Ops:
  6.5 0.0 copy-start
  6.5 0.0 copy-start.1
  6.5 0.0 all-gather.3.cloned.1.call-start
  6.5 0.7 all-gather.3.cloned.1.call-update
  7.3 1.0 %fusion.13 = f32[128]{0:T(128)S(1)} fusion(bf16[128,768]{1,0:T(8,128)(2,1)} %param.10), kind=kLoop, calls=%fused_computation.19 | loop fusion | flops 294784 | bytes 197120 | tf_op jit(solution)/shard_map/reduce_sum | solution.py:23
  8.3 0.0 copy-done
  8.3 1.3 %convolution_convert_fusion.1 = bf16[128,768]{1,0:T(8,128)(2,1)S(1)} fusion(bf16[768,768]{1,0:T(8,128)(2,1)S(1)} %copy-done, bf16[128,768]{1,0:T(8,128)(2,1)} %param.10, f32[768]{0:T(1024)} %param.13, f32[128]{0:T(128)S(1)} %add_rsqrt_fusion.1), kind=kOutput, calls=%fused_computation.9 | convolution fusion | flops 151486464 | bytes 1576448 | tf_op jit(solution)/shard_map/dot_general | solution.py:63
  9.6 0.2 copy.28
  9.8 0.7 convert_element_type.108
  10.5 1.1 %copy.39 = bf16[256,512]{0,1:T(8,128)(2,1)S(1)} copy(bf16[256,512]{1,0:T(8,128)(2,1)} %param.17) | data formatting | bytes 524288 | tf_op jit(solution)/shard_map/reshape | solution.py:106
  11.6 0.1 fusion.36
  11.8 0.1 pad_maximum_fusion
  11.8 24.3 %all_gather.17 = bf16[512,64]{1,0:T(8,128)(2,1)S(1)} all-gather(bf16[32,64]{1,0:T(8,128)(2,1)S(1)} %pad_maximum_fusion), channel_id=1, replica_groups=mesh['grp'=2,'sp'=4,'tp'=4] {'sp','tp'}, dimensions={0}, use_global_device_ids=true | all-gather | bytes 69632 | tf_op jit(solution)/shard_map/all_gather | solution.py:75
  36.2 0.8 fusion.28
  37.0 0.8 fusion.30
  37.8 20.0 %all_gather.16 = bf16[512,256]{1,0:T(8,128)(2,1)S(1)} all-gather(bf16[32,256]{1,0:T(8,128)(2,1)S(1)} %fusion.30), channel_id=1, replica_groups=mesh['grp'=2,'sp'=4,'tp'=4] {'sp','tp'}, dimensions={0}, use_global_device_ids=true | all-gather | bytes 278528 | tf_op jit(solution)/shard_map/all_gather | solution.py:74
  57.9 0.1 multiply_cosine_fusion.1
  58.0 0.0 copy-done.1
  58.1 0.3 convolution_convert_fusion
  58.4 0.0 copy-start.2
  58.4 0.3 convolution_bitcast_fusion
  58.8 0.3 fusion.41
  59.1 0.2 fusion.7
  59.2 0.6 multiply_reduce_fusion
  59.8 0.1 copy.34
  59.9 0.0 copy-done.2
  60.0 7.3 %all_gather.18 = bf16[4,128,512]{2,1,0:T(8,128)(2,1)S(1)} all-gather(bf16[1,128,512]{2,1,0:T(8,128)(2,1)S(1)} %multiply_convert_fusion), channel_id=1, replica_groups=mesh['grp'=2,'sp'=4,'tp'=4] {'tp'}, dimensions={0}, use_global_device_ids=true | all-gather | bytes 655360 | tf_op jit(solution)/shard_map/all_gather | solution.py:16
  67.3 0.3 copy.35
  67.5 5.1 %all-gather = bf16[4,1,128]{2,1,0:T(2,128)(2,1)S(1)} all-gather(bf16[1,1,128]{2,1,0:T(2,128)(2,1)S(1)} %bitcast.38), channel_id=1, replica_groups=mesh['grp'=2,'sp'=4,'tp'=4] {'tp'}, dimensions={0}, use_global_device_ids=true | all-gather | bytes 1280 | tf_op jit(solution)/shard_map/all_gather | solution.py:116
  72.6 20.8 %all-gather.3.cloned.1.call-done = bf16[2048,1024]{1,0:T(8,128)(2,1)} async-done(((bf16[512,1024]{1,0:T(8,128)(2,1)}), bf16[2048,1024]{1,0:T(8,128)(2,1)}) %all-gather.3.cloned.1.call-update) | async-done | bytes 4194320 | tf_op jit(solution)/shard_map/all_gather | solution.py:123
  93.5 3.6 %fusion.3 = bf16[128,1024]{1,0:T(8,128)(2,1)} fusion(bf16[128,2048]{0,1:T(8,128)(2,1)S(1)} %bitcast.32, bf16[2048,1024]{1,0:T(8,128)(2,1)} %all-gather.3.cloned.1.call-done, f32[128]{0:T(128)S(1)} %add_rsqrt_fusion), kind=kOutput, calls=%fused_computation.8 | convolution fusion | flops 537133056 | bytes 4981248 | tf_op jit(solution)/shard_map/dot_general | solution.py:121
  (12 shorter events, 0.1 us)
Async XLA Ops:
  6.5 1.8 %copy-start = (bf16[768,768]{1,0:T(8,128)(2,1)S(1)}, bf16[768,768]{1,0:T(8,128)(2,1)}, u32[]{:S(2)}) copy-start(bf16[768,768]{1,0:T(8,128)(2,1)} %param.15) | copy-start | bytes 3538948
  6.5 51.5 %copy-start.1 = (bf16[256,512]{1,0:T(8,128)(2,1)S(1)}, bf16[256,512]{1,0:T(8,128)(2,1)}, u32[]{:S(2)}) copy-start(bf16[256,512]{1,0:T(8,128)(2,1)} %param.16) | copy-start | bytes 786436
  6.5 86.9 %all-gather.3.cloned.1.call-start = ((), (), s32[]{:S(2)}) async-start(), calls=%async_computation | async-start | bytes 5242880 | tf_op jit(solution)/shard_map/all_gather | solution.py:123
  58.4 1.5 %copy-start.2 = (f32[512]{0:T(512)S(1)}, f32[512]{0:T(512)}, u32[]{:S(2)}) copy-start(f32[512]{0:T(512)} %param.18) | copy-start | bytes 6148
Sparse Core Ops, SparseCore 0:
  8.9 84.5 all-gather.2
